TPU v7x, 32 devices: a whole 2x2x4 slice. The times are simulated.
32 devices in a mesh: grp: 2 (over x), tp: 4 (over y, core), dp: 4 (over z).
Axes of the slice: x: 2, y: 2, z: 4, core: 2. Of those that a mesh axis runs over, the one named last changes fastest.
Arguments:
- tokens: bfloat16 [512, 2048], P(('grp', 'tp'), 'dp'), parts along dimension 0, may hold values from -25 to 25
- state: float32 [2, 512, 16, 128, 128], P(None, ('grp', 'dp'), 'tp'), parts along dimension 1, may hold values from -1 to 1
- lengths: int32 [512], P(('grp', 'dp')), parts along dimension 0, may hold values from 1 to 4096, 131072 in all
- norm_gain: bfloat16 [2, 2048], P(None, 'dp'), may hold values from 0.099609375 to 1.8984375
- w_query: bfloat16 [2, 2048, 2048], P(None, 'dp', 'tp'), may hold values from -0.125 to 0.125
- w_forget: bfloat16 [2, 2048, 2048], P(None, 'dp', 'tp'), may hold values from -0.125 to 0.125
- w_input: bfloat16 [2, 2048, 2048], P(None, 'dp', 'tp'), may hold values from -0.125 to 0.125
- w_gate: bfloat16 [2, 2048, 2048], P(None, 'dp', 'tp'), may hold values from -0.125 to 0.125
- w_out: bfloat16 [2, 2048, 2048], P(None, 'tp', 'dp'), may hold values from -0.125 to 0.125
- bound_logit: float32 [2, 2048], P(None, 'tp'), may hold values from -3 to 5
- pace: float32 [2, 2048], P(None, 'tp'), may hold values from 0.6 to 2
- head_gain: float32 [2, 128], replicated, may hold values from 0.4 to 2.5
Outputs:
- mixed: float32 [512, 2048], P(('grp', 'tp'), 'dp'), parts along dimension 0
- new_state: float32 [2, 512, 16, 128, 128], P(None, ('grp', 'dp'), 'tp'), parts along dimension 1
There are 2 independent parts, one for each index of `grp`. A program takes and returns all parts, laid end to end along the dimension named above; an argument that names none is the same for every part. Nothing has to cross between parts.
All inputs are finite; a program needn't handle non-finite values. No bound on the sum of `lengths` on one device may be relied on, other than what follows from the above.
Results may differ from a plain program's by a relative error of at most 0.0083.
Values may be sent and summed in bfloat16 or wider, within the bound.
A program may use at most 192 MiB of HBM per device.

v0:
```python
import jax
import jax.numpy as jnp
from jax import lax
from jax.sharding import PartitionSpec as P

D = 2048
LENGTH_MEAN = 512
epsilon = 1e-06


def advance(prior, query, forget_in, value, gate, lower, pace_row, log_len, gain_row):
    count, width = query.shape
    size = prior.shape[-1]
    heads = width // size
    pre = forget_in - pace_row[None, :] * log_len[:, None]
    forget = lower[None, :] + (1.0 - lower[None, :]) * jax.nn.sigmoid(pre)
    key = (1.0 - lower[None, :]) * jax.nn.sigmoid(-pre)
    forget = forget.reshape(count, heads, size)
    key = key.reshape(count, heads, size)
    values = value.reshape(count, heads, size)
    updated = forget[..., None] * prior + key[..., None] * values[:, :, None, :]
    readout = jnp.einsum(
        "bhk,bhkv->bhv", query.reshape(count, heads, size), updated, precision=lax.Precision.HIGHEST
    )
    normed = readout * lax.rsqrt(jnp.mean(readout * readout, axis=-1, keepdims=True) + epsilon)
    gates = gate.reshape(count, heads, size)
    normed = normed * gain_row[None, None, :] * jax.nn.silu(gates)
    return (updated, normed.reshape(count, width).astype(jnp.bfloat16))


def shards(
    tokens,
    state,
    lengths,
    norm_gain,
    w_query,
    w_forget,
    w_input,
    w_gate,
    w_out,
    bound_logit,
    pace,
    head_gain,
):
    current = tokens
    log_len = jnp.log(lengths.astype(jnp.float32) / LENGTH_MEAN)
    own_count = state.shape[1]
    states = []
    result = None
    for block in range(2):
        whole = lax.all_gather(current, "tp", axis=0, tiled=True)
        whole_wide = whole.astype(jnp.float32)
        partial_sq = jnp.sum(whole_wide * whole_wide, axis=1)
        squares_all = lax.psum(partial_sq, "dp")
        squares = lax.dynamic_slice_in_dim(
            squares_all, lax.axis_index("dp") * own_count, own_count, 0
        )
        gained = (whole_wide * norm_gain[block].astype(jnp.float32)[None, :]).astype(jnp.bfloat16)
        terms = tuple(
            (
                jnp.dot(gained, weight[block], preferred_element_type=jnp.float32)
                for weight in (w_query, w_forget, w_input, w_gate)
            )
        )
        sums = lax.psum_scatter(terms, "dp", scatter_dimension=0, tiled=True)
        scale = lax.rsqrt(squares / D + epsilon)
        made = [scale[:, None] * total for total in sums]
        lower = jax.nn.sigmoid(bound_logit[block])
        updated, normed = advance(
            state[block],
            made[0],
            made[1],
            made[2],
            made[3],
            lower,
            pace[block],
            log_len,
            head_gain[block],
        )
        states.append(updated)
        gathered = lax.all_gather(normed, "dp", axis=0, tiled=True)
        out_weight = w_out[block]
        branch = lax.psum_scatter(
            jnp.dot(gathered, out_weight, preferred_element_type=jnp.float32),
            "tp",
            scatter_dimension=0,
            tiled=True,
        )
        if block == 0:
            current = (current.astype(jnp.float32) + branch).astype(jnp.bfloat16)
        else:
            result = current.astype(jnp.float32) + branch
    return (result, jnp.stack(states))


def solution(mesh):
    in_specs = (
        P(("grp", "tp"), "dp"),
        P(None, ("grp", "dp"), "tp", None, None),
        P(("grp", "dp")),
        P(None, "dp"),
        P(None, "dp", "tp"),
        P(None, "dp", "tp"),
        P(None, "dp", "tp"),
        P(None, "dp", "tp"),
        P(None, "tp", "dp"),
        P(None, "tp"),
        P(None, "tp"),
        P(),
    )
    out_specs = (P(("grp", "tp"), "dp"), P(None, ("grp", "dp"), "tp", None, None))
    return jax.shard_map(shards, mesh=mesh, in_specs=in_specs, out_specs=out_specs, check_vma=False)
```

profile of v0, /device:TPU:0, one launch (start us, length us, event | category | flops | bytes accessed | tf_op | source)
XLA Modules:
  0.0 361.6 jit_solution(16375477499638168452)
XLA Ops:
  7.2 0.8 slice_convert_fusion
  8.0 7.4 %all_gather.12 = bf16[256,512]{1,0:T(8,128)(2,1)S(1)} all-gather(bf16[64,512]{1,0:T(8,128)(2,1)} %param.12), channel_id=1, replica_groups=mesh['grp'=2,'tp'=4,'dp'=4] {'tp'}, dimensions={0}, use_global_device_ids=true | all-gather | bytes 327680 | tf_op jit(solution)/shard_map/all_gather | solution.py:51
  15.4 2.1 fusion.36
  17.6 2.1 fusion.34
  19.8 2.2 fusion.32
  22.1 2.2 fusion.38
  24.3 0.1 fusion.16
  24.5 12.0 %psum.14 = f32[256]{0:T(256)S(1)} all-reduce(f32[256]{0:T(256)S(1)} %fusion.16), channel_id=1, replica_groups=mesh['grp'=2,'tp'=4,'dp'=4] {'dp'}, use_global_device_ids=true, to_apply=%region_1.0 | all-reduce | flops 256 | bytes 2048 | tf_op jit(solution)/shard_map/psum | solution.py:54
  36.4 0.1 add_rsqrt_fusion.3
  36.5 0.7 multiply_log_fusion
  37.2 1.3 slice_bitcast_fusion
  38.5 0.8 fusion.62
  39.3 0.8 broadcast_subtract_fusion
  40.1 0.8 reduce-scatter.13.cloned.1.call-done
  40.9 22.4 %reduce-scatter.15.cloned.1.call-done = f32[64,512]{1,0:T(8,128)} async-done(((f32[256,512]{1,0:T(8,128)}), f32[64,512]{1,0:T(8,128)}) %reduce-scatter.15.cloned.1.call-update) | async-done | bytes 131088 | tf_op jit(solution)/shard_map/reduce_scatter | solution.py:65
  63.4 22.4 %reduce-scatter.17.cloned.1.call-done = f32[64,512]{1,0:T(8,128)} async-done(((f32[256,512]{1,0:T(8,128)}), f32[64,512]{1,0:T(8,128)}) %reduce-scatter.17.cloned.1.call-update) | async-done | bytes 131088 | tf_op jit(solution)/shard_map/reduce_scatter | solution.py:65
  85.8 22.2 %reduce-scatter.11.cloned.1.call-done = f32[64,512]{1,0:T(8,128)} async-done(((f32[256,512]{1,0:T(8,128)}), f32[64,512]{1,0:T(8,128)}) %reduce-scatter.11.cloned.1.call-update) | async-done | bytes 131088 | tf_op jit(solution)/shard_map/reduce_scatter | solution.py:65
  108.0 1.2 multiply_add_fusion.3
  109.5 0.7 reshape.56
  110.2 0.7 reshape.61
  110.9 22.7 %fusion.4 = f32[64,4,1,128]{3,2,1,0:T(1,128)S(1)} fusion(f32[64,4,128,1]{2,3,1,0:T(1,128)} %bitcast.79, f32[2,64,4,128,128]{4,3,2,1,0:T(8,128)} %param.13, f32[64,4,128]{2,1,0:T(4,128)S(1)} %mul.316, f32[64,4,128]{2,1,0:T(4,128)S(1)} %mul.313, f32[64,4,128]{2,1,0:T(4,128)S(1)} %mul.309), kind=kOutput, calls=%fused_computation.6 | convolution fusion | flops 62914560 | bytes 17432576 | tf_op jit(solution)/shard_map/bhk,bhkv->bhv/dot_general | solution.py:22
  133.6 0.1 multiply_reduce_fusion.1
  133.8 0.1 fusion.61
  134.0 13.8 %all_gather.13 = bf16[256,512]{1,0:T(8,128)(2,1)S(1)} all-gather(bf16[64,512]{1,0:T(8,128)(2,1)S(1)} %bitcast.74), channel_id=1, replica_groups=mesh['grp'=2,'tp'=4,'dp'=4] {'dp'}, dimensions={0}, use_global_device_ids=true | all-gather | bytes 327680 | tf_op jit(solution)/shard_map/all_gather | solution.py:81
  147.8 2.1 fusion.30
  150.0 19.9 %reduce-scatter.19.cloned.1.call-done = f32[64,512]{1,0:T(8,128)} async-done(((f32[256,512]{1,0:T(8,128)}), f32[64,512]{1,0:T(8,128)}) %reduce-scatter.19.cloned.1.call-update) | async-done | bytes 131088 | tf_op jit(solution)/shard_map/reduce_scatter | solution.py:83
  169.9 0.9 add_convert_fusion
  170.9 5.8 %all_gather.14 = bf16[256,512]{1,0:T(8,128)(2,1)S(1)} all-gather(bf16[64,512]{1,0:T(8,128)(2,1)S(1)} %add_convert_fusion), channel_id=1, replica_groups=mesh['grp'=2,'tp'=4,'dp'=4] {'tp'}, dimensions={0}, use_global_device_ids=true | all-gather | bytes 327680 | tf_op jit(solution)/shard_map/all_gather | solution.py:51
  176.7 1.1 fusion.26
  177.8 1.1 fusion.24
  179.0 1.1 fusion.22
  180.2 2.2 fusion.28
  182.4 0.1 fusion.18
  182.6 11.7 %psum.15 = f32[256]{0:T(256)S(1)} all-reduce(f32[256]{0:T(256)S(1)} %fusion.18), channel_id=1, replica_groups=mesh['grp'=2,'tp'=4,'dp'=4] {'dp'}, use_global_device_ids=true, to_apply=%region_9.10 | all-reduce | flops 256 | bytes 2048 | tf_op jit(solution)/shard_map/psum | solution.py:54
  194.3 0.1 add_rsqrt_fusion.2
  194.4 5.5 %reduce-scatter.23.cloned.1.call-done = f32[64,512]{1,0:T(8,128)} async-done(((f32[256,512]{1,0:T(8,128)}), f32[64,512]{1,0:T(8,128)}) %reduce-scatter.23.cloned.1.call-update) | async-done | bytes 131088 | tf_op jit(solution)/shard_map/reduce_scatter | solution.py:65
  199.9 22.4 %reduce-scatter.25.cloned.1.call-done = f32[64,512]{1,0:T(8,128)} async-done(((f32[256,512]{1,0:T(8,128)}), f32[64,512]{1,0:T(8,128)}) %reduce-scatter.25.cloned.1.call-update) | async-done | bytes 131088 | tf_op jit(solution)/shard_map/reduce_scatter | solution.py:65
  222.3 22.4 %reduce-scatter.27.cloned.1.call-done = f32[64,512]{1,0:T(8,128)} async-done(((f32[256,512]{1,0:T(8,128)}), f32[64,512]{1,0:T(8,128)}) %reduce-scatter.27.cloned.1.call-update) | async-done | bytes 131088 | tf_op jit(solution)/shard_map/reduce_scatter | solution.py:65
  244.7 22.4 %reduce-scatter.21.cloned.1.call-done = f32[64,512]{1,0:T(8,128)} async-done(((f32[256,512]{1,0:T(8,128)}), f32[64,512]{1,0:T(8,128)}) %reduce-scatter.21.cloned.1.call-update) | async-done | bytes 131088 | tf_op jit(solution)/shard_map/reduce_scatter | solution.py:65
  267.1 1.2 multiply_add_fusion.2
  268.6 23.2 %multiply_add_fusion.1 = (f32[1,64,4,128,128]{4,3,2,1,0:T(8,128)}, f32[1,64,4,128,128]{4,3,2,1,0:T(8,128)}) fusion(f32[2,64,4,128,128]{4,3,2,1,0:T(8,128)} %param.13, f32[64,4,128]{2,1,0:T(4,128)} %copy-done.6, f32[64,4,128]{2,1,0:T(4,128)} %copy-done.5, f32[64,4,128]{2,1,0:T(4,128)} %copy-done.4, f32[64,4,128]{2,1,0:T(4,128)S(1)} %mul.349, ...), kind=kLoop, calls=%fused_computation.8 | loop fusion | flops 25165824 | bytes 67895296 | tf_op jit(solution)/shard_map/add | solution.py:21
  291.8 22.6 %fusion.1 = f32[64,4,1,128]{3,2,1,0:T(1,128)S(1)} fusion(f32[64,4,128,1]{2,3,1,0:T(1,128)S(1)} %bitcast.78, f32[2,64,4,128,128]{4,3,2,1,0:T(8,128)} %param.13, f32[64,4,128]{2,1,0:T(4,128)S(1)} %mul.349, f32[64,4,128]{2,1,0:T(4,128)S(1)} %mul.346, f32[64,4,128]{2,1,0:T(4,128)S(1)} %mul.342), kind=kOutput, calls=%fused_computation.3 | convolution fusion | flops 62914560 | bytes 17432576 | tf_op jit(solution)/shard_map/bhk,bhkv->bhv/dot_general | solution.py:22
  314.4 0.1 multiply_reduce_fusion
  314.6 0.1 fusion.60
  314.8 13.8 %all_gather.15 = bf16[256,512]{1,0:T(8,128)(2,1)S(1)} all-gather(bf16[64,512]{1,0:T(8,128)(2,1)S(1)} %bitcast.75), channel_id=1, replica_groups=mesh['grp'=2,'tp'=4,'dp'=4] {'dp'}, dimensions={0}, use_global_device_ids=true | all-gather | bytes 327680 | tf_op jit(solution)/shard_map/all_gather | solution.py:81
  328.6 1.1 fusion.20
  329.7 23.4 %pad_maximum_fusion = f32[2,64,4,128,128]{4,3,2,1,0:T(8,128)} fusion(f32[1,64,4,128,128]{4,3,2,1,0:T(8,128)} %get-tuple-element.7, f32[1,64,4,128,128]{4,3,2,1,0:T(8,128)} %get-tuple-element.6), kind=kLoop, calls=%fused_computation | loop fusion | flops 8388608 | bytes 67108864 | tf_op jit(solution)/shard_map/stack | solution.py:93
  353.1 1.6 convert_add_fusion
  (55 shorter events, 1.1 us)
Async XLA Ops:
  7.2 33.7 %reduce-scatter.13.cloned.1.call-start = ((), (), s32[]{:S(2)}) async-start(), calls=%async_computation.11 | async-start | bytes 655360 | tf_op jit(solution)/shard_map/reduce_scatter | solution.py:65
  17.6 45.8 %reduce-scatter.15.cloned.1.call-start = ((), (), s32[]{:S(2)}) async-start(), calls=%async_computation.12 | async-start | bytes 655360 | tf_op jit(solution)/shard_map/reduce_scatter | solution.py:65
  19.8 66.0 %reduce-scatter.17.cloned.1.call-start = ((), (), s32[]{:S(2)}) async-start(), calls=%async_computation.13 | async-start | bytes 655360 | tf_op jit(solution)/shard_map/reduce_scatter | solution.py:65
  22.0 86.0 %reduce-scatter.11.cloned.1.call-start = ((), (), s32[]{:S(2)}) async-start(), calls=%async_computation.10 | async-start | bytes 655360 | tf_op jit(solution)/shard_map/reduce_scatter | solution.py:65
  24.3 145.7 %reduce-scatter.19.cloned.1.call-start = ((), (), s32[]{:S(2)}) async-start(), calls=%async_computation.14 | async-start | bytes 655360 | tf_op jit(solution)/shard_map/reduce_scatter | solution.py:83
  37.2 73.7 %copy-start.8 = (f32[64]{0:T(128)}, f32[64]{0:T(128)S(1)}, u32[]{:S(2)}) copy-start(f32[64]{0:T(128)S(1)} %multiply_log_fusion) | copy-start | bytes 772
  109.3 24.6 %copy-start.4 = (f32[64,4,128]{2,1,0:T(4,128)}, f32[64,4,128]{2,1,0:T(4,128)S(1)}, u32[]{:S(2)}) copy-start(f32[64,4,128]{2,1,0:T(4,128)S(1)} %mul.309) | copy-start | bytes 393220
  109.4 24.6 %copy-start.5 = (f32[64,4,128]{2,1,0:T(4,128)}, f32[64,4,128]{2,1,0:T(4,128)S(1)}, u32[]{:S(2)}) copy-start(f32[64,4,128]{2,1,0:T(4,128)S(1)} %mul.313) | copy-start | bytes 393220
  109.5 40.5 %copy-start.6 = (f32[64,4,128]{2,1,0:T(4,128)}, f32[64,4,128]{2,1,0:T(4,128)S(1)}, u32[]{:S(2)}) copy-start(f32[64,4,128]{2,1,0:T(4,128)S(1)} %mul.316) | copy-start | bytes 393220
  110.9 22.9 %copy-start.7 = (f32[64,4,128]{2,1,0:T(4,128)S(1)}, f32[64,4,128]{2,1,0:T(4,128)}, u32[]{:S(2)}) copy-start(f32[64,4,128]{2,1,0:T(4,128)} %reshape.56) | copy-start | bytes 393220
  110.9 22.9 %copy-start.10 = (f32[128]{0:T(128)S(1)}, f32[128]{0:T(128)}, u32[]{:S(2)}) copy-start(f32[128]{0:T(128)} %get-tuple-element.19) | copy-start | bytes 1540
  110.9 65.8 %copy-start = (bf16[2,512,512]{2,1,0:T(8,128)(2,1)S(1)}, bf16[2,512,512]{2,1,0:T(8,128)(2,1)}, u32[]{:S(2)}) copy-start(bf16[2,512,512]{2,1,0:T(8,128)(2,1)} %param.17) | copy-start | bytes 3145732
  110.9 66.9 %copy-start.1 = (bf16[2,512,512]{2,1,0:T(8,128)(2,1)S(1)}, bf16[2,512,512]{2,1,0:T(8,128)(2,1)}, u32[]{:S(2)}) copy-start(bf16[2,512,512]{2,1,0:T(8,128)(2,1)} %param.18) | copy-start | bytes 3145732
  110.9 68.1 %copy-start.2 = (bf16[2,512,512]{2,1,0:T(8,128)(2,1)S(1)}, bf16[2,512,512]{2,1,0:T(8,128)(2,1)}, u32[]{:S(2)}) copy-start(bf16[2,512,512]{2,1,0:T(8,128)(2,1)} %param.19) | copy-start | bytes 3145732
  150.0 49.9 %reduce-scatter.23.cloned.1.call-start = ((), (), s32[]{:S(2)}) async-start(), calls=%async_computation.16 | async-start | bytes 655360 | tf_op jit(solution)/shard_map/reduce_scatter | solution.py:65
  177.8 44.5 %reduce-scatter.25.cloned.1.call-start = ((), (), s32[]{:S(2)}) async-start(), calls=%async_computation.17 | async-start | bytes 655360 | tf_op jit(solution)/shard_map/reduce_scatter | solution.py:65
  178.9 65.7 %reduce-scatter.27.cloned.1.call-start = ((), (), s32[]{:S(2)}) async-start(), calls=%async_computation.18 | async-start | bytes 655360 | tf_op jit(solution)/shard_map/reduce_scatter | solution.py:65
  180.1 86.9 %reduce-scatter.21.cloned.1.call-start = ((), (), s32[]{:S(2)}) async-start(), calls=%async_computation.15 | async-start | bytes 655360 | tf_op jit(solution)/shard_map/reduce_scatter | solution.py:65
  182.4 170.8 %reduce-scatter.29.cloned.1.call-start = ((), (), s32[]{:S(2)}) async-start(), calls=%async_computation.19 | async-start | bytes 655360 | tf_op jit(solution)/shard_map/reduce_scatter | solution.py:83
  291.8 22.8 %copy-start.9 = (f32[128]{0:T(128)S(1)}, f32[128]{0:T(128)}, u32[]{:S(2)}) copy-start(f32[128]{0:T(128)} %get-tuple-element.18) | copy-start | bytes 1540
  291.8 36.8 %copy-start.3 = (bf16[2,512,512]{2,1,0:T(8,128)(2,1)S(1)}, bf16[2,512,512]{2,1,0:T(8,128)(2,1)}, u32[]{:S(2)}) copy-start(bf16[2,512,512]{2,1,0:T(8,128)(2,1)} %param.20) | copy-start | bytes 3145732
Sparse Core Ops, SparseCore 0:
  17.7 23.1 reduce-scatter.12
  43.2 20.1 reduce-scatter.14
  65.6 20.1 reduce-scatter.16
  87.9 20.0 reduce-scatter.10
  150.1 19.8 reduce-scatter.18
  177.9 21.9 reduce-scatter.22
  202.2 20.0 reduce-scatter.24
  224.6 20.0 reduce-scatter.26
  247.0 20.0 reduce-scatter.20
  329.8 19.8 reduce-scatter.28
where the time goes:
time: 362 us
  waiting for transfers between devices  161 us (44%)
  blocking collectives  64.5 us (18%)
  matrix products  62.6 us (17%)
  other arithmetic  54.8 us (15%)
  between operations  14.5 us (4%)
  local copies, waits for them, and re-layouts  3.97 us (1%)
    reduce_scatter x8, waiting for transfers between devices, shards(): sums = lax.psum_scatter(terms, 'dp', scatter_dimension=0, tiled=True)  141 us
    dot_general x2, matrix products, advance(): jnp.einsum('bhk,bhkv->bhv', query.reshape(count, heads, size), updated, p...  45.3 us
    all_gather x2, blocking collectives, shards(): gathered = lax.all_gather(normed, 'dp', axis=0, tiled=True)  27.6 us
    psum x2, blocking collectives, shards(): squares_all = lax.psum(partial_sq, 'dp')  23.7 us
    another operation x1, other arithmetic, shards(): return (result, jnp.stack(states))  23.4 us
    add x1, other arithmetic, advance(): updated = forget[..., None] * prior + key[..., None] * values[:, :, None, :]  23.2 us
    reduce_scatter x2, waiting for transfers between devices, shards(): lax.psum_scatter(jnp.dot(gathered, out_weight, preferred_element_type=jnp...  19.9 us
    dot_general x8, matrix products, shards(): jnp.dot(gained, weight[block], preferred_element_type=jnp.float32)  14.1 us
  transfers between devices with their start and end apart: 10, of which 9 were waited for; matrix products, arithmetic and copies ran while one was open for 11% of the time, Pallas kernels for 0%

commit v1 on v0

--- a/solution.py
+++ b/solution.py
@@ -51,7 +51,7 @@
         whole = lax.all_gather(current, "tp", axis=0, tiled=True)
         whole_wide = whole.astype(jnp.float32)
         partial_sq = jnp.sum(whole_wide * whole_wide, axis=1)
-        squares_all = lax.psum(partial_sq, "dp")
+        squares_all = jnp.sum(lax.all_gather(partial_sq, "dp"), axis=0)
         squares = lax.dynamic_slice_in_dim(
             squares_all, lax.axis_index("dp") * own_count, own_count, 0
         )

time: 362 us -> 362 us (level)
    psum x2 -> x0, blocking collectives: 23.7 us -> none  [shards(): squares_all = lax.psum(partial_sq, 'dp')]
    all_gather x0 -> x2, blocking collectives: none -> 22.3 us  [shards(): squares_all = jnp.sum(lax.all_gather(partial_sq, 'dp'), axis=0)]
where the time goes in v1:
time: 362 us; the launch traced here: 361 us
  waiting for transfers between devices  162 us (45%)
  blocking collectives  63.2 us (17%)
  matrix products  62.6 us (17%)
  other arithmetic  54.9 us (15%)
  between operations  14.5 us (4%)
  local copies, waits for them, and re-layouts  3.97 us (1%)
    reduce_scatter x8, waiting for transfers between devices, shards(): sums = lax.psum_scatter(terms, 'dp', scatter_dimension=0, tiled=True)  142 us
    dot_general x2, matrix products, advance(): jnp.einsum('bhk,bhkv->bhv', query.reshape(count, heads, size), updated, p...  45.3 us
    all_gather x2, blocking collectives, shards(): gathered = lax.all_gather(normed, 'dp', axis=0, tiled=True)  27.7 us
    another operation x1, other arithmetic, shards(): return (result, jnp.stack(states))  23.4 us
    add x1, other arithmetic, advance(): updated = forget[..., None] * prior + key[..., None] * values[:, :, None, :]  23.2 us
    all_gather x2, blocking collectives, shards(): squares_all = jnp.sum(lax.all_gather(partial_sq, 'dp'), axis=0)  22.3 us
    reduce_scatter x2, waiting for transfers between devices, shards(): lax.psum_scatter(jnp.dot(gathered, out_weight, preferred_element_type=jnp...  19.8 us
    dot_general x8, matrix products, shards(): jnp.dot(gained, weight[block], preferred_element_type=jnp.float32)  14.1 us
  transfers between devices with their start and end apart: 10, of which 9 were waited for; matrix products, arithmetic and copies ran while one was open for 11% of the time, Pallas kernels for 0%

profile of v1, /device:TPU:0, one launch (start us, length us, event | category | flops | bytes accessed | tf_op | source)
XLA Modules:
  0.0 361.3 jit_solution(12222880513553631090)
XLA Ops:
  7.2 0.8 slice_convert_fusion
  8.0 7.4 %all_gather.24 = bf16[256,512]{1,0:T(8,128)(2,1)S(1)} all-gather(bf16[64,512]{1,0:T(8,128)(2,1)} %param.12), channel_id=1, replica_groups=mesh['grp'=2,'tp'=4,'dp'=4] {'tp'}, dimensions={0}, use_global_device_ids=true | all-gather | bytes 327680 | tf_op jit(solution)/shard_map/all_gather | solution.py:51
  15.4 2.1 fusion.36
  17.6 2.1 fusion.34
  19.8 2.2 fusion.32
  22.1 2.2 fusion.38
  24.3 0.1 fusion.16
  24.5 11.4 %all-gather.2 = f32[4,1,256]{2,1,0:T(1,128)S(1)} all-gather(f32[1,1,256]{2,1,0:T(1,128)S(1)} %bitcast.96), channel_id=2, replica_groups=mesh['grp'=2,'tp'=4,'dp'=4] {'dp'}, dimensions={0}, use_global_device_ids=true | all-gather | bytes 5120 | tf_op jit(solution)/shard_map/all_gather | solution.py:54
  35.8 0.1 add_rsqrt_fusion.3
  35.9 0.7 multiply_log_fusion
  36.6 1.3 slice_bitcast_fusion
  37.9 0.8 fusion.62
  38.7 0.8 broadcast_subtract_fusion
  39.5 1.3 reduce-scatter.13.cloned.1.call-done
  40.8 22.5 %reduce-scatter.15.cloned.1.call-done = f32[64,512]{1,0:T(8,128)} async-done(((f32[256,512]{1,0:T(8,128)}), f32[64,512]{1,0:T(8,128)}) %reduce-scatter.15.cloned.1.call-update) | async-done | bytes 131088 | tf_op jit(solution)/shard_map/reduce_scatter | solution.py:65
  63.3 22.4 %reduce-scatter.17.cloned.1.call-done = f32[64,512]{1,0:T(8,128)} async-done(((f32[256,512]{1,0:T(8,128)}), f32[64,512]{1,0:T(8,128)}) %reduce-scatter.17.cloned.1.call-update) | async-done | bytes 131088 | tf_op jit(solution)/shard_map/reduce_scatter | solution.py:65
  85.7 22.3 %reduce-scatter.11.cloned.1.call-done = f32[64,512]{1,0:T(8,128)} async-done(((f32[256,512]{1,0:T(8,128)}), f32[64,512]{1,0:T(8,128)}) %reduce-scatter.11.cloned.1.call-update) | async-done | bytes 131088 | tf_op jit(solution)/shard_map/reduce_scatter | solution.py:65
  108.0 1.2 multiply_add_fusion.3
  109.5 0.7 reshape.56
  110.2 0.7 reshape.69
  110.9 22.7 %fusion.4 = f32[64,4,1,128]{3,2,1,0:T(1,128)S(1)} fusion(f32[64,4,128,1]{2,3,1,0:T(1,128)} %bitcast.81, f32[2,64,4,128,128]{4,3,2,1,0:T(8,128)} %param.13, f32[64,4,128]{2,1,0:T(4,128)S(1)} %mul.316, f32[64,4,128]{2,1,0:T(4,128)S(1)} %mul.313, f32[64,4,128]{2,1,0:T(4,128)S(1)} %mul.309), kind=kOutput, calls=%fused_computation.6 | convolution fusion | flops 62914560 | bytes 17432576 | tf_op jit(solution)/shard_map/bhk,bhkv->bhv/dot_general | solution.py:22
  133.6 0.1 multiply_reduce_fusion.1
  133.8 0.1 fusion.61
  134.0 13.9 %all_gather.27 = bf16[256,512]{1,0:T(8,128)(2,1)S(1)} all-gather(bf16[64,512]{1,0:T(8,128)(2,1)S(1)} %bitcast.76), channel_id=1, replica_groups=mesh['grp'=2,'tp'=4,'dp'=4] {'dp'}, dimensions={0}, use_global_device_ids=true | all-gather | bytes 327680 | tf_op jit(solution)/shard_map/all_gather | solution.py:81
  147.8 2.1 fusion.30
  150.1 19.8 %reduce-scatter.19.cloned.1.call-done = f32[64,512]{1,0:T(8,128)} async-done(((f32[256,512]{1,0:T(8,128)}), f32[64,512]{1,0:T(8,128)}) %reduce-scatter.19.cloned.1.call-update) | async-done | bytes 131088 | tf_op jit(solution)/shard_map/reduce_scatter | solution.py:83
  169.9 0.9 add_convert_fusion
  170.8 5.8 %all_gather.28 = bf16[256,512]{1,0:T(8,128)(2,1)S(1)} all-gather(bf16[64,512]{1,0:T(8,128)(2,1)S(1)} %add_convert_fusion), channel_id=1, replica_groups=mesh['grp'=2,'tp'=4,'dp'=4] {'tp'}, dimensions={0}, use_global_device_ids=true | all-gather | bytes 327680 | tf_op jit(solution)/shard_map/all_gather | solution.py:51
  176.6 1.1 fusion.26
  177.8 1.1 fusion.24
  178.9 1.1 fusion.22
  180.1 2.2 fusion.28
  182.4 0.1 fusion.18
  182.5 10.9 %all-gather.3 = f32[4,1,256]{2,1,0:T(1,128)S(1)} all-gather(f32[1,1,256]{2,1,0:T(1,128)S(1)} %bitcast.97), channel_id=3, replica_groups=mesh['grp'=2,'tp'=4,'dp'=4] {'dp'}, dimensions={0}, use_global_device_ids=true | all-gather | bytes 5120 | tf_op jit(solution)/shard_map/all_gather | solution.py:54
  193.5 0.1 add_rsqrt_fusion.2
  193.5 6.2 %reduce-scatter.23.cloned.1.call-done = f32[64,512]{1,0:T(8,128)} async-done(((f32[256,512]{1,0:T(8,128)}), f32[64,512]{1,0:T(8,128)}) %reduce-scatter.23.cloned.1.call-update) | async-done | bytes 131088 | tf_op jit(solution)/shard_map/reduce_scatter | solution.py:65
  199.7 22.3 %reduce-scatter.25.cloned.1.call-done = f32[64,512]{1,0:T(8,128)} async-done(((f32[256,512]{1,0:T(8,128)}), f32[64,512]{1,0:T(8,128)}) %reduce-scatter.25.cloned.1.call-update) | async-done | bytes 131088 | tf_op jit(solution)/shard_map/reduce_scatter | solution.py:65
  222.1 22.4 %reduce-scatter.27.cloned.1.call-done = f32[64,512]{1,0:T(8,128)} async-done(((f32[256,512]{1,0:T(8,128)}), f32[64,512]{1,0:T(8,128)}) %reduce-scatter.27.cloned.1.call-update) | async-done | bytes 131088 | tf_op jit(solution)/shard_map/reduce_scatter | solution.py:65
  244.4 22.4 %reduce-scatter.21.cloned.1.call-done = f32[64,512]{1,0:T(8,128)} async-done(((f32[256,512]{1,0:T(8,128)}), f32[64,512]{1,0:T(8,128)}) %reduce-scatter.21.cloned.1.call-update) | async-done | bytes 131088 | tf_op jit(solution)/shard_map/reduce_scatter | solution.py:65
  266.8 1.3 multiply_add_fusion.2
  268.4 23.2 %multiply_add_fusion.1 = (f32[1,64,4,128,128]{4,3,2,1,0:T(8,128)}, f32[1,64,4,128,128]{4,3,2,1,0:T(8,128)}) fusion(f32[2,64,4,128,128]{4,3,2,1,0:T(8,128)} %param.13, f32[64,4,128]{2,1,0:T(4,128)} %copy-done.6, f32[64,4,128]{2,1,0:T(4,128)} %copy-done.5, f32[64,4,128]{2,1,0:T(4,128)} %copy-done.4, f32[64,4,128]{2,1,0:T(4,128)S(1)} %mul.349, ...), kind=kLoop, calls=%fused_computation.8 | loop fusion | flops 25165824 | bytes 67895296 | tf_op jit(solution)/shard_map/add | solution.py:21
  291.6 22.6 %fusion.1 = f32[64,4,1,128]{3,2,1,0:T(1,128)S(1)} fusion(f32[64,4,128,1]{2,3,1,0:T(1,128)S(1)} %bitcast.80, f32[2,64,4,128,128]{4,3,2,1,0:T(8,128)} %param.13, f32[64,4,128]{2,1,0:T(4,128)S(1)} %mul.349, f32[64,4,128]{2,1,0:T(4,128)S(1)} %mul.346, f32[64,4,128]{2,1,0:T(4,128)S(1)} %mul.342), kind=kOutput, calls=%fused_computation.3 | convolution fusion | flops 62914560 | bytes 17432576 | tf_op jit(solution)/shard_map/bhk,bhkv->bhv/dot_general | solution.py:22
  314.2 0.1 multiply_reduce_fusion
  314.4 0.1 fusion.60
  314.6 13.8 %all_gather.31 = bf16[256,512]{1,0:T(8,128)(2,1)S(1)} all-gather(bf16[64,512]{1,0:T(8,128)(2,1)S(1)} %bitcast.77), channel_id=1, replica_groups=mesh['grp'=2,'tp'=4,'dp'=4] {'dp'}, dimensions={0}, use_global_device_ids=true | all-gather | bytes 327680 | tf_op jit(solution)/shard_map/all_gather | solution.py:81
  328.4 1.1 fusion.20
  329.5 23.4 %pad_maximum_fusion = f32[2,64,4,128,128]{4,3,2,1,0:T(8,128)} fusion(f32[1,64,4,128,128]{4,3,2,1,0:T(8,128)} %get-tuple-element.7, f32[1,64,4,128,128]{4,3,2,1,0:T(8,128)} %get-tuple-element.6), kind=kLoop, calls=%fused_computation | loop fusion | flops 8388608 | bytes 67108864 | tf_op jit(solution)/shard_map/stack | solution.py:93
  352.9 1.6 convert_add_fusion
  (57 shorter events, 1.1 us)
Async XLA Ops:
  7.2 33.6 %reduce-scatter.13.cloned.1.call-start = ((), (), s32[]{:S(2)}) async-start(), calls=%async_computation.11 | async-start | bytes 655360 | tf_op jit(solution)/shard_map/reduce_scatter | solution.py:65
  17.6 45.7 %reduce-scatter.15.cloned.1.call-start = ((), (), s32[]{:S(2)}) async-start(), calls=%async_computation.12 | async-start | bytes 655360 | tf_op jit(solution)/shard_map/reduce_scatter | solution.py:65
  19.8 65.9 %reduce-scatter.17.cloned.1.call-start = ((), (), s32[]{:S(2)}) async-start(), calls=%async_computation.13 | async-start | bytes 655360 | tf_op jit(solution)/shard_map/reduce_scatter | solution.py:65
  22.0 86.0 %reduce-scatter.11.cloned.1.call-start = ((), (), s32[]{:S(2)}) async-start(), calls=%async_computation.10 | async-start | bytes 655360 | tf_op jit(solution)/shard_map/reduce_scatter | solution.py:65
  24.3 145.6 %reduce-scatter.19.cloned.1.call-start = ((), (), s32[]{:S(2)}) async-start(), calls=%async_computation.14 | async-start | bytes 655360 | tf_op jit(solution)/shard_map/reduce_scatter | solution.py:83
  36.6 74.3 %copy-start.8 = (f32[64]{0:T(128)}, f32[64]{0:T(128)S(1)}, u32[]{:S(2)}) copy-start(f32[64]{0:T(128)S(1)} %multiply_log_fusion) | copy-start | bytes 772
  109.3 24.6 %copy-start.4 = (f32[64,4,128]{2,1,0:T(4,128)}, f32[64,4,128]{2,1,0:T(4,128)S(1)}, u32[]{:S(2)}) copy-start(f32[64,4,128]{2,1,0:T(4,128)S(1)} %mul.309) | copy-start | bytes 393220
  109.4 24.6 %copy-start.5 = (f32[64,4,128]{2,1,0:T(4,128)}, f32[64,4,128]{2,1,0:T(4,128)S(1)}, u32[]{:S(2)}) copy-start(f32[64,4,128]{2,1,0:T(4,128)S(1)} %mul.313) | copy-start | bytes 393220
  109.4 40.6 %copy-start.6 = (f32[64,4,128]{2,1,0:T(4,128)}, f32[64,4,128]{2,1,0:T(4,128)S(1)}, u32[]{:S(2)}) copy-start(f32[64,4,128]{2,1,0:T(4,128)S(1)} %mul.316) | copy-start | bytes 393220
  110.9 22.9 %copy-start.7 = (f32[64,4,128]{2,1,0:T(4,128)S(1)}, f32[64,4,128]{2,1,0:T(4,128)}, u32[]{:S(2)}) copy-start(f32[64,4,128]{2,1,0:T(4,128)} %reshape.56) | copy-start | bytes 393220
  110.9 22.9 %copy-start.10 = (f32[128]{0:T(128)S(1)}, f32[128]{0:T(128)}, u32[]{:S(2)}) copy-start(f32[128]{0:T(128)} %get-tuple-element.19) | copy-start | bytes 1540
  110.9 65.7 %copy-start = (bf16[2,512,512]{2,1,0:T(8,128)(2,1)S(1)}, bf16[2,512,512]{2,1,0:T(8,128)(2,1)}, u32[]{:S(2)}) copy-start(bf16[2,512,512]{2,1,0:T(8,128)(2,1)} %param.17) | copy-start | bytes 3145732
  110.9 66.9 %copy-start.1 = (bf16[2,512,512]{2,1,0:T(8,128)(2,1)S(1)}, bf16[2,512,512]{2,1,0:T(8,128)(2,1)}, u32[]{:S(2)}) copy-start(bf16[2,512,512]{2,1,0:T(8,128)(2,1)} %param.18) | copy-start | bytes 3145732
  110.9 68.1 %copy-start.2 = (bf16[2,512,512]{2,1,0:T(8,128)(2,1)S(1)}, bf16[2,512,512]{2,1,0:T(8,128)(2,1)}, u32[]{:S(2)}) copy-start(bf16[2,512,512]{2,1,0:T(8,128)(2,1)} %param.19) | copy-start | bytes 3145732
  150.0 49.7 %reduce-scatter.23.cloned.1.call-start = ((), (), s32[]{:S(2)}) async-start(), calls=%async_computation.16 | async-start | bytes 655360 | tf_op jit(solution)/shard_map/reduce_scatter | solution.py:65
  177.7 44.3 %reduce-scatter.25.cloned.1.call-start = ((), (), s32[]{:S(2)}) async-start(), calls=%async_computation.17 | async-start | bytes 655360 | tf_op jit(solution)/shard_map/reduce_scatter | solution.py:65
  178.9 65.6 %reduce-scatter.27.cloned.1.call-start = ((), (), s32[]{:S(2)}) async-start(), calls=%async_computation.18 | async-start | bytes 655360 | tf_op jit(solution)/shard_map/reduce_scatter | solution.py:65
  180.1 86.8 %reduce-scatter.21.cloned.1.call-start = ((), (), s32[]{:S(2)}) async-start(), calls=%async_computation.15 | async-start | bytes 655360 | tf_op jit(solution)/shard_map/reduce_scatter | solution.py:65
  182.3 170.6 %reduce-scatter.29.cloned.1.call-start = ((), (), s32[]{:S(2)}) async-start(), calls=%async_computation.19 | async-start | bytes 655360 | tf_op jit(solution)/shard_map/reduce_scatter | solution.py:83
  291.6 22.8 %copy-start.9 = (f32[128]{0:T(128)S(1)}, f32[128]{0:T(128)}, u32[]{:S(2)}) copy-start(f32[128]{0:T(128)} %get-tuple-element.18) | copy-start | bytes 1540
  291.6 36.8 %copy-start.3 = (bf16[2,512,512]{2,1,0:T(8,128)(2,1)S(1)}, bf16[2,512,512]{2,1,0:T(8,128)(2,1)}, u32[]{:S(2)}) copy-start(bf16[2,512,512]{2,1,0:T(8,128)(2,1)} %param.20) | copy-start | bytes 3145732
Sparse Core Ops, SparseCore 0:
  17.7 23.0 reduce-scatter.12
  43.0 20.2 reduce-scatter.14
  65.6 20.1 reduce-scatter.16
  87.9 20.1 reduce-scatter.10
  150.1 19.7 reduce-scatter.18
  177.8 21.8 reduce-scatter.22
  202.0 20.0 reduce-scatter.24
  224.3 20.0 reduce-scatter.26
  246.7 20.0 reduce-scatter.20
  329.6 19.8 reduce-scatter.28
